TPU v7x, 32 devices: a whole 2x2x4 slice. The times are simulated.
32 devices in a mesh: sp: 8 (over z, y), tp: 4 (over x, core).
Axes of the slice: x: 2, y: 2, z: 4, core: 2. Of those that a mesh axis runs over, the one named last changes fastest.
Arguments:
- resid: bfloat16 [2048, 2048], P(('sp', 'tp')), may hold values from -6 to 6
- queries: bfloat16 [2048, 1024], P('sp', 'tp'), may hold values from -6 to 6
- keys: bfloat16 [2048, 256], P('sp', 'tp'), may hold values from -6 to 6
- values: bfloat16 [2048, 256], P('sp', 'tp'), may hold values from -6 to 6
- docs: int32 [2048], P('sp'), may hold values from 0 to 3, never falling along the last dimension, each value on 1 to 1024 neighbouring positions
- q_gain: float32 [64], replicated, may hold values from 0.1 to 1.9
- key_norm_gain: float32 [64], replicated, may hold values from 0.1 to 1.9
- sink: float32 [16], P('tp'), may hold values from 4 to 8
- out_gain: float32 [1024], replicated, may hold values from 0.1 to 1.9
- w_out: bfloat16 [1024, 2048], replicated, may hold values from -0.1875 to 0.1875
- norm_gain: float32 [2048], replicated, may hold values from 0.1 to 1.9
- routes: int32 [2048, 4], P('sp'), may hold values from 0 to 7, all different within a row; in each aligned block of 64 rows (0 to 63, 64 to 127, ...) at most 50 rows name the same one
- route_weights: float32 [2048, 4], P(('sp', 'tp')), may hold values from 0.1 to 1
- w_gate: bfloat16 [8, 2048, 2048], P('sp', None, 'tp'), may hold values from -0.375 to 0.375
- w_up: bfloat16 [8, 2048, 2048], P('sp', None, 'tp'), may hold values from -0.375 to 0.375
- w_down: bfloat16 [8, 2048, 2048], P('sp', 'tp'), may hold values from -0.015625 to 0.015625
Outputs:
- layer_out: bfloat16 [2048, 2048], P(('sp', 'tp'))
Inputs may be any that keep to these rules, and one draw needn't show every extreme that they name: `routes`: in each aligned block of 64 tokens no expert is named more than 50 times, and some expert is named exactly that often; the 4 experts of a token differ. `docs`: document numbers never fall along the sequence, and each document has 1 to 1024 positions.
All inputs are finite; a program needn't handle non-finite values.
Results may differ from a plain program's by a relative error of at most 0.015.
Values may be sent and summed in bfloat16 or wider, within the bound.
A program may use at most 128 MiB of HBM per device.

v0:
```python
import functools

import jax
import jax.numpy as jnp
from jax import lax
from jax.experimental import pallas as pl
from jax.experimental.pallas import tpu as pltpu
from jax.sharding import PartitionSpec as P

WINDOW = 128


rope_base = 10000.0
norm_eps = 1e-06
swiglu_limit = 7.0
swiglu_alpha = 1.702


def row_normalize(values, gain_vec):
    floats = values.astype(jnp.float32)
    scale_inv = lax.rsqrt(jnp.mean(floats * floats, axis=-1, keepdims=True) + norm_eps)
    return floats * scale_inv * gain_vec


def apply_rotary_heads(heads, token_positions):
    half_size = heads.shape[-1] // 2
    freqs = rope_base ** (-jnp.arange(half_size, dtype=jnp.float32) / half_size)
    angles = token_positions[:, None] * freqs[None, :]
    cosine = jnp.cos(angles)[:, None, :]
    sine = jnp.sin(angles)[:, None, :]
    first_half = heads[..., :half_size]
    second_half = heads[..., half_size:]
    return jnp.concatenate(
        [first_half * cosine - second_half * sine, first_half * sine + second_half * cosine],
        axis=-1,
    )


def expert_act(gate_pre, up_pre):
    gate_cut = jnp.minimum(gate_pre, swiglu_limit)
    up_cut = jnp.clip(up_pre, -swiglu_limit, swiglu_limit)
    return (up_cut + 1.0) * gate_cut * jax.nn.sigmoid(swiglu_alpha * gate_cut)


def slot_tables(route_block, expert_count, capacity):
    pair_total = route_block.shape[1]
    expert_ids = jnp.arange(expert_count, dtype=jnp.int32)
    onehot = (route_block[:, :, None] == expert_ids[None, None, :]).astype(jnp.int32)
    before = jnp.cumsum(onehot, axis=1) - onehot
    rank = jnp.sum(before * onehot, axis=-1)
    pair_slot = route_block * capacity + rank
    slot_ids = jnp.arange(expert_count * capacity, dtype=jnp.int32)
    match = pair_slot[:, :, None] == slot_ids[None, None, :]
    pair_ids = jnp.arange(pair_total, dtype=jnp.int32)
    slot_pair = jnp.sum(jnp.where(match, pair_ids[None, :, None], 0), axis=1)
    filled = jnp.any(match, axis=1)
    return (pair_slot, slot_pair, filled)


def expert_partial(arrived_rows, w_gate, w_up, w_down):
    lead_shape = arrived_rows.shape
    local_experts = w_gate.shape[0]
    grouped = arrived_rows.reshape(-1, local_experts, lead_shape[2] // local_experts, lead_shape[3])
    gate_pre = jnp.einsum("recd,edf->recf", grouped, w_gate, preferred_element_type=jnp.float32)
    up_pre = jnp.einsum("recd,edf->recf", grouped, w_up, preferred_element_type=jnp.float32)
    hidden = expert_act(gate_pre, up_pre).astype(jnp.bfloat16)
    partial_value = jnp.einsum("recf,efd->recd", hidden, w_down, preferred_element_type=jnp.float32)
    return (
        lax.optimization_barrier(partial_value.astype(jnp.bfloat16))
        .astype(jnp.float32)
        .reshape(lead_shape)
    )


LANES = 128
VMEM_LIMIT = 60 * 1024 * 1024
MESH = pl.DeviceIdType.MESH


def moe_kernel(
    zn, x_in, wg_hbm, wu_hbm, wd_hbm, out,
    X, S, P1, crecv, rx, ry, rdx, rdy, zl, zr, acc, wg, wu, wd,
    wsem, ag_s, ag_r, c_s, c_r, rs_s, rs_r,
):
    sp, tp = lax.axis_index("sp"), lax.axis_index("tp")
    z, y = sp // 2, sp % 2
    xx, c = tp // 2, tp % 2
    T, W = x_in.shape
    D = out.shape[1]
    H = D // 2
    F = wg.shape[1]
    right, left = (sp + 2, tp), (sp - 2, tp)
    ynb = (z * 2 + (1 - y), tp)
    xnb = (sp, (1 - xx) * 2 + c)
    cnb = (sp, xx * 2 + (1 - c))
    has_r, has_l = z < zn - 1, z > 0

    loads = [
        pltpu.make_async_copy(src.at[0], dst, wsem.at[i])
        for i, (src, dst) in enumerate(((wg_hbm, wg), (wu_hbm, wu), (wd_hbm, wd)))
    ]
    for load in loads:
        load.start()

    bar = pltpu.get_barrier_semaphore()
    for nb in (ynb, xnb, cnb):
        pl.semaphore_signal(bar, inc=1, device_id=nb, device_id_type=MESH)

    @pl.when(has_r)
    def _():
        pl.semaphore_signal(bar, inc=1, device_id=right, device_id_type=MESH)

    @pl.when(has_l)
    def _():
        pl.semaphore_signal(bar, inc=1, device_id=left, device_id_type=MESH)

    peers = 3 + (z < zn - 1).astype(jnp.int32) + (z > 0).astype(jnp.int32)
    pl.semaphore_wait(bar, peers)

    def rows(zz):
        return pl.ds(pl.multiple_of(zz * T, T), T)

    def rc(src, dst, ss, rs, dev):
        return pltpu.make_async_remote_copy(
            src_ref=src, dst_ref=dst, send_sem=ss, recv_sem=rs, device_id=dev, device_id_type=MESH
        )

    A, B = pl.ds(0, H), pl.ds(H, W - H)

    def ag(kind, zz, own=False):
        table = {
            "zr": (0, 0, None, right), "zl": (0, 0, None, left),
            "y": (0, 1, None, ynb), "x": (0, 2, None, xnb),
            "xa": (1, 3, A, xnb), "yb": (2, 3, B, ynb),
            "c0": (0, 4, None, cnb), "c1": (1, 5, None, cnb),
            "c2": (2, 6, None, cnb), "c3": (3, 7, None, cnb),
        }
        k = list(table).index(kind)
        sg, dg, cols, dev = table[kind]
        r = rows(zz)
        if cols is None:
            src, dst = X.at[sg, r], X.at[dg, r]
        else:
            src, dst = X.at[sg, r, cols], X.at[dg, r, cols]
        if own:
            src = x_in
        return rc(src, dst, ag_s.at[k, zz], ag_r.at[k, zz], dev)

    def each(fn, order):
        for s in order:
            if s == 0:
                fn(z, 0, 0)
            else:
                for side in (-1, 1):
                    zz = z + side * s
                    valid = (zz >= 0) & (zz < zn)

                    @pl.when(valid)
                    def _(zz=zz, s=s, side=side):
                        fn(zz, s, side)

    X[0, rows(z)] = x_in[...]

    def first(zz, s, side):
        own = s == 0
        if side == -1:
            ag("zr", zz).wait_recv()
        if side == 1:
            ag("zl", zz).wait_recv()
        if side <= 0:
            @pl.when(has_r)
            def _():
                ag("zr", zz, own).start()
        if side >= 0:
            @pl.when(has_l)
            def _():
                ag("zl", zz, own).start()
        for k in ("y", "x", "c0"):
            ag(k, zz, own).start()

    def second(zz, s, side):
        ag("y", zz).wait_recv()
        ag("xa", zz).start()
        ag("c1", zz).start()
        ag("x", zz).wait_recv()
        ag("yb", zz).start()
        ag("c2", zz).start()

    def third(zz, s, side):
        ag("xa", zz).wait_recv()
        ag("yb", zz).wait_recv()
        ag("c3", zz).start()

    def group_core(q):
        return rc(P1.at[q], crecv.at[q], c_s.at[q], c_r.at[q], cnb)

    def expert(g):
        xg = X[g, :, pl.ds(0, D)]
        gate = jnp.dot(xg, wg[...], preferred_element_type=jnp.float32)
        up = jnp.dot(xg, wu[...], preferred_element_type=jnp.float32)
        h = expert_act(gate, up).astype(jnp.bfloat16)
        tail = X[g, :, pl.ds(D, LANES)].astype(jnp.float32)
        lane = lax.broadcasted_iota(jnp.int32, tail.shape, 1)
        weight = jnp.sum(jnp.where(lane % (2 * zn) == sp, tail, 0.0), axis=1, keepdims=True)
        q = g % 4
        if g < 4:
            group_core(q).wait_recv()
        step = F
        for n in range(0, D, step):
            cols = pl.ds(n, step)
            part = jnp.dot(h, wd[:, cols], preferred_element_type=jnp.float32) * weight
            if g < 4:
                S[q, :, cols] = (part + crecv[q, :, cols].astype(jnp.float32)).astype(jnp.bfloat16)
            else:
                P1[q, :, cols] = part.astype(jnp.bfloat16)

    def core_arrivals(k):
        for zz in range(zn):
            ag(k, zz).wait_recv()

    lo, hi = pl.ds(0, H), pl.ds(H, H)

    def rs(kind, zz):
        r = rows(zz)
        table = {
            "yb": (S.at[1, r, hi], ry.at[r, hi], ynb),
            "xa": (S.at[2, r, lo], rx.at[r, lo], xnb),
            "dxa": (S.at[3, r, lo], rdx.at[r], xnb),
            "dyb": (S.at[3, r, hi], rdy.at[r], ynb),
            "ya": (S.at[1, r, lo], ry.at[r, lo], ynb),
            "xb": (S.at[2, r, hi], rx.at[r, hi], xnb),
            "zr": (S.at[0, r], zl.at[r], right),
            "zl": (S.at[0, r], zr.at[r], left),
        }
        k = list(table).index(kind)
        src, dst, dev = table[kind]
        return rc(src, dst, rs_s.at[k, zz], rs_r.at[k, zz], dev)

    far = list(range(zn - 1, -1, -1))
    near = list(range(zn))

    for s in range(zn):
        each(first, [s])
        if s > 0:
            each(second, [s - 1])
    each(second, [zn - 1])
    for load in loads:
        load.wait()
    core_arrivals("c1")
    expert(5)
    group_core(1).start()
    expert(1)
    each(lambda zz, s, side: rs("yb", zz).start(), far)
    core_arrivals("c2")
    expert(6)
    group_core(2).start()
    expert(2)
    each(lambda zz, s, side: rs("xa", zz).start(), far)
    each(third, near)
    core_arrivals("c3")
    expert(7)
    group_core(3).start()
    expert(3)

    def diag(zz, s, side):
        rs("dxa", zz).start()
        rs("dyb", zz).start()

    each(diag, far)
    core_arrivals("c0")
    expert(4)
    group_core(0).start()
    expert(0)

    f32 = jnp.float32

    def mid_sums(zz, s, side):
        r = rows(zz)
        rs("dxa", zz).wait_recv()
        S[1, r, lo] = (S[1, r, lo].astype(f32) + rdx[r].astype(f32)).astype(jnp.bfloat16)
        rs("ya", zz).start()
        rs("dyb", zz).wait_recv()
        S[2, r, hi] = (S[2, r, hi].astype(f32) + rdy[r].astype(f32)).astype(jnp.bfloat16)
        rs("xb", zz).start()

    def last_sums(zz, s, side):
        r = rows(zz)
        for k in ("xa", "xb", "ya", "yb"):
            rs(k, zz).wait_recv()
        acc[...] = S[0, r].astype(f32) + rx[r].astype(f32) + ry[r].astype(f32)
        if side >= 0:
            @pl.when(has_l)
            def _():
                rs("zr", zz).wait_recv()
                acc[...] += zl[r].astype(f32)
        if side <= 0:
            @pl.when(has_r)
            def _():
                rs("zl", zz).wait_recv()
                acc[...] += zr[r].astype(f32)
        if s == 0:
            out[...] = acc[...]
        else:
            S[0, r] = acc[...].astype(jnp.bfloat16)
            if side == 1:
                rs("zr", zz).start()
            else:
                rs("zl", zz).start()

    for i, s in enumerate(far):
        each(mid_sums, [s])
        if i > 0:
            each(last_sums, [far[i - 1]])
    each(last_sums, [far[-1]])

    def drain(zz, s, side):
        own = s == 0
        if side <= 0:
            @pl.when(has_r)
            def _():
                ag("zr", zz, own).wait_send()
        if side >= 0:
            @pl.when(has_l)
            def _():
                ag("zl", zz, own).wait_send()
        for k in ("y", "x", "c0"):
            ag(k, zz, own).wait_send()
        for k in ("xa", "yb", "c1", "c2", "c3"):
            ag(k, zz).wait_send()
        for k in ("yb", "xa", "dxa", "dyb", "ya", "xb"):
            rs(k, zz).wait_send()
        if side == 1:
            rs("zr", zz).wait_send()
        if side == -1:
            rs("zl", zz).wait_send()

    each(drain, near)
    for q in range(4):
        group_core(q).wait_send()


def moe_exchange(x_in, w_gate, w_up, w_down):
    zn = lax.axis_size("sp") // 2
    T, W = x_in.shape
    D = w_gate.shape[1]
    F = w_gate.shape[2]
    G = zn * T
    bf = jnp.bfloat16
    vm = pl.BlockSpec(memory_space=pltpu.VMEM)
    anyspec = pl.BlockSpec(memory_space=pl.ANY)
    return pl.pallas_call(
        functools.partial(moe_kernel, zn),
        out_shape=jax.ShapeDtypeStruct((T, D), jnp.float32),
        in_specs=[vm, anyspec, anyspec, anyspec],
        out_specs=vm,
        scratch_shapes=[
            pltpu.VMEM((8, G, W), bf),
            pltpu.VMEM((4, G, D), bf),
            pltpu.VMEM((4, G, D), bf),
            pltpu.VMEM((4, G, D), bf),
            pltpu.VMEM((G, D), bf),
            pltpu.VMEM((G, D), bf),
            pltpu.VMEM((G, D // 2), bf),
            pltpu.VMEM((G, D // 2), bf),
            pltpu.VMEM((G, D), bf),
            pltpu.VMEM((G, D), bf),
            pltpu.VMEM((T, D), jnp.float32),
            pltpu.VMEM((D, F), bf),
            pltpu.VMEM((D, F), bf),
            pltpu.VMEM((F, D), bf),
            pltpu.SemaphoreType.DMA((3,)),
            pltpu.SemaphoreType.DMA((10, zn)),
            pltpu.SemaphoreType.DMA((10, zn)),
            pltpu.SemaphoreType.DMA((4,)),
            pltpu.SemaphoreType.DMA((4,)),
            pltpu.SemaphoreType.DMA((8, zn)),
            pltpu.SemaphoreType.DMA((8, zn)),
        ],
        compiler_params=pltpu.CompilerParams(
            collective_id=1, has_side_effects=True, vmem_limit_bytes=VMEM_LIMIT
        ),
        name="moe_exchange",
    )(x_in, w_gate, w_up, w_down)


def dense_fits(tokens, width, sp_size, tp_size, local_experts, hidden):
    experts = sp_size * local_experts
    gathered = tokens * (width + LANES) * 2
    buffers = gathered + tokens * width * 4 + 3 * hidden * width * 2
    return (
        tp_size == 4
        and sp_size % 2 == 0
        and local_experts == 1
        and 2 * experts <= LANES
        and width % (2 * LANES) == 0
        and width % hidden == 0
        and buffers < VMEM_LIMIT * 3 // 5
    )


def row_weights(own_routes, route_weights, expert_count):
    ids = jnp.arange(expert_count, dtype=jnp.int32)
    hit = own_routes[:, :, None] == ids[None, None, :]
    dense = jnp.sum(jnp.where(hit, route_weights[:, :, None], 0.0), axis=1)
    top = lax.reduce_precision(dense, 8, 7)
    low = dense - top
    both = jnp.concatenate([top, low], axis=1).astype(jnp.bfloat16)
    return jnp.pad(both, ((0, 0), (0, LANES - 2 * expert_count)))


def halo_kernel(peers, width, x, out, before, after, ss, rs):
    sp, tp = lax.axis_index("sp"), lax.axis_index("tp")
    length = x.shape[0]
    up, down = (sp + 1, tp), (sp - 1, tp)
    has_up, has_down = sp < peers - 1, sp > 0
    bar = pltpu.get_barrier_semaphore()

    def send(part, dst, i, dev):
        return pltpu.make_async_remote_copy(
            src_ref=part, dst_ref=dst, send_sem=ss.at[i], recv_sem=rs.at[i],
            device_id=dev, device_id_type=MESH,
        )

    go_up = send(x.at[pl.ds(length - width, width)], before, 0, up)
    go_down = send(x.at[pl.ds(0, width)], after, 1, down)

    @pl.when(has_up)
    def _():
        pl.semaphore_signal(bar, inc=1, device_id=up, device_id_type=MESH)

    @pl.when(has_down)
    def _():
        pl.semaphore_signal(bar, inc=1, device_id=down, device_id_type=MESH)

    pl.semaphore_wait(bar, has_up.astype(jnp.int32) + has_down.astype(jnp.int32))

    @pl.when(has_up)
    def _():
        go_up.start()

    @pl.when(has_down)
    def _():
        go_down.start()

    out[pl.ds(width, length)] = x[...]
    edge = jnp.zeros(before.shape, before.dtype)

    @pl.when(has_down)
    def _():
        go_up.wait_recv()
        out[pl.ds(0, width)] = before[...]

    @pl.when(jnp.logical_not(has_down))
    def _():
        out[pl.ds(0, width)] = edge

    @pl.when(has_up)
    def _():
        go_down.wait_recv()
        out[pl.ds(length + width, width)] = after[...]

    @pl.when(jnp.logical_not(has_up))
    def _():
        out[pl.ds(length + width, width)] = edge

    @pl.when(has_up)
    def _():
        go_up.wait_send()

    @pl.when(has_down)
    def _():
        go_down.wait_send()


def halo(x, width):
    length, columns = x.shape
    vm = pl.BlockSpec(memory_space=pltpu.VMEM)
    return pl.pallas_call(
        functools.partial(halo_kernel, lax.axis_size("sp"), width),
        out_shape=jax.ShapeDtypeStruct((length + 2 * width, columns), x.dtype),
        in_specs=[vm],
        out_specs=vm,
        scratch_shapes=[
            pltpu.VMEM((width, columns), x.dtype),
            pltpu.VMEM((width, columns), x.dtype),
            pltpu.SemaphoreType.DMA((2,)),
            pltpu.SemaphoreType.DMA((2,)),
        ],
        compiler_params=pltpu.CompilerParams(collective_id=2, has_side_effects=True),
        name="halo",
    )(x)


def swap_kernel(n, x, out, held, ss, rs):
    sp, me = lax.axis_index("sp"), lax.axis_index("tp")
    q, columns = out.shape[0], x.shape[1]
    bar = pltpu.get_barrier_semaphore()
    for p in range(1, n):
        pl.semaphore_signal(bar, inc=1, device_id=(sp, (me + p) % n), device_id_type=MESH)
    pl.semaphore_wait(bar, n - 1)

    def send(p):
        to = (me + p) % n
        part = pl.ds(pl.multiple_of(to * q, q), q)
        return pltpu.make_async_remote_copy(
            src_ref=x.at[part], dst_ref=held.at[me], send_sem=ss.at[p], recv_sem=rs.at[me],
            device_id=(sp, to), device_id_type=MESH,
        )

    for p in range(1, n):
        send(p).start()
    for s in range(n):
        cols = pl.ds(s * columns, columns)

        @pl.when(me == s)
        def _(cols=cols):
            out[:, cols] = x[pl.ds(pl.multiple_of(me * q, q), q)]

        @pl.when(me != s)
        def _(cols=cols, s=s):
            pltpu.make_async_remote_copy(
                src_ref=held.at[s], dst_ref=held.at[s], send_sem=ss.at[0], recv_sem=rs.at[s],
                device_id=(sp, (me + 1) % n), device_id_type=MESH,
            ).wait_recv()
            out[:, cols] = held[s]
    for p in range(1, n):
        send(p).wait_send()


def swap(x):
    n = lax.axis_size("tp")
    length, columns = x.shape
    vm = pl.BlockSpec(memory_space=pltpu.VMEM)
    return pl.pallas_call(
        functools.partial(swap_kernel, n),
        out_shape=jax.ShapeDtypeStruct((length // n, n * columns), x.dtype),
        in_specs=[vm],
        out_specs=vm,
        scratch_shapes=[
            pltpu.VMEM((n, length // n, columns), x.dtype),
            pltpu.SemaphoreType.DMA((n,)),
            pltpu.SemaphoreType.DMA((n,)),
        ],
        compiler_params=pltpu.CompilerParams(collective_id=3, has_side_effects=True),
        name="swap",
    )(x)


def per_device(
    resid,
    queries,
    keys,
    values,
    docs,
    q_gain,
    key_norm_gain,
    sink,
    out_gain,
    w_out,
    norm_gain,
    routes,
    route_weights,
    w_gate,
    w_up,
    w_down,
):
    sp_size = lax.axis_size("sp")
    tp_size = lax.axis_size("tp")
    sp_index = lax.axis_index("sp")
    tp_index = lax.axis_index("tp")
    tok_rows = queries.shape[0]
    head_size = q_gain.shape[0]
    query_heads = sink.shape[0]
    kv_heads = keys.shape[1] // head_size
    query_group_width = query_heads // kv_heads
    token_positions = (sp_index * tok_rows + jnp.arange(tok_rows, dtype=jnp.int32)).astype(
        jnp.float32
    )
    q_rot = apply_rotary_heads(
        row_normalize(queries.reshape(tok_rows, query_heads, head_size), q_gain), token_positions
    ).astype(jnp.bfloat16)
    key_rotated = apply_rotary_heads(
        row_normalize(keys.reshape(tok_rows, kv_heads, head_size), key_norm_gain), token_positions
    ).astype(jnp.bfloat16)
    key_value = jnp.concatenate(
        [key_rotated.reshape(tok_rows, kv_heads * head_size), values], axis=1
    )
    doc_mark = (docs + 1).astype(jnp.bfloat16)
    kv_width = key_value.shape[1]
    marks = jnp.broadcast_to(doc_mark[:, None], (tok_rows, LANES))
    packed_span = halo(jnp.concatenate([key_value, marks], axis=1), WINDOW)
    kv_span, doc_span = packed_span[:, :kv_width], packed_span[:, kv_width]
    span_rows = tok_rows + 2 * WINDOW
    k_span = kv_span[:, : kv_heads * head_size].reshape(span_rows, kv_heads, head_size)
    v_span = kv_span[:, kv_heads * head_size :].reshape(span_rows, kv_heads, head_size)
    scores = jnp.einsum(
        "qhgd,khd->hgqk",
        q_rot.reshape(tok_rows, kv_heads, query_group_width, head_size),
        k_span,
        preferred_element_type=jnp.float32,
    ) * head_size ** (-0.5)
    offsets = jnp.arange(tok_rows, dtype=jnp.int32)[:, None] - (
        jnp.arange(span_rows, dtype=jnp.int32)[None, :] - WINDOW
    )
    allowed = (jnp.abs(offsets) <= WINDOW) & (doc_mark[:, None] == doc_span[None, :])
    raw_weights = jnp.where(allowed[None, None], jnp.exp(scores), jnp.zeros((), jnp.float32))
    sink_exponent = jnp.exp(sink).reshape(kv_heads, query_group_width)
    total = jnp.sum(raw_weights, axis=-1) + sink_exponent[:, :, None]
    probs = (raw_weights / total[..., None]).astype(jnp.bfloat16)
    att = jnp.einsum("hgqk,khd->qhgd", probs, v_span, preferred_element_type=jnp.float32)
    att = att.astype(jnp.bfloat16).reshape(tok_rows, query_heads * head_size)
    by_token = swap(att)
    att_normed = row_normalize(by_token, out_gain).astype(jnp.bfloat16)
    middle = (
        resid.astype(jnp.float32) + jnp.dot(att_normed, w_out, preferred_element_type=jnp.float32)
    ).astype(jnp.bfloat16)
    moe_in = row_normalize(middle, norm_gain).astype(jnp.bfloat16)
    quarter = tok_rows // tp_size
    top_count = routes.shape[1]
    local_experts = w_gate.shape[0]
    expert_count = sp_size * local_experts
    capacity = 3 * quarter * top_count // (2 * expert_count) + 2
    model_width = moe_in.shape[1]
    empty = jnp.zeros((), jnp.bfloat16)
    own_routes = lax.dynamic_slice_in_dim(routes, tp_index * quarter, quarter, 0)
    if dense_fits(
        tok_rows * sp_size, model_width, sp_size, tp_size, local_experts, w_gate.shape[2]
    ):
        tail = row_weights(own_routes, route_weights, expert_count)
        packed = jnp.concatenate([moe_in, tail], axis=1)
        routed = moe_exchange(packed, w_gate, w_up, w_down)
        return (middle.astype(jnp.float32) + routed).astype(jnp.bfloat16)
    pair_slot, slot_pair, filled = slot_tables(
        own_routes.reshape(1, quarter * top_count), expert_count, capacity
    )
    outgoing = jnp.where(filled[:, :, None], moe_in[slot_pair // top_count], empty)
    outgoing = outgoing.reshape(1, sp_size, local_experts * capacity, model_width)
    arrived = lax.all_to_all(outgoing, "sp", split_axis=1, concat_axis=1, tiled=True)
    terms = expert_partial(lax.all_gather(arrived, "tp", axis=0, tiled=True), w_gate, w_up, w_down)
    summed = lax.psum_scatter(terms.astype(jnp.bfloat16), "tp", scatter_dimension=0, tiled=True)
    own_slot = pair_slot[0]
    returned = lax.all_to_all(summed, "sp", split_axis=1, concat_axis=1, tiled=True)
    picked = returned.reshape(-1, model_width)[own_slot].reshape(quarter, top_count, model_width)
    routed = jnp.sum(picked.astype(jnp.float32) * route_weights[:, :, None], axis=1)
    return (middle.astype(jnp.float32) + routed).astype(jnp.bfloat16)


def solution(mesh):
    return jax.shard_map(
        per_device,
        mesh=mesh,
        in_specs=(
            P(("sp", "tp"), None),
            P("sp", "tp"),
            P("sp", "tp"),
            P("sp", "tp"),
            P("sp"),
            P(),
            P(),
            P("tp"),
            P(),
            P(),
            P(),
            P("sp", None),
            P(("sp", "tp"), None),
            P("sp", None, "tp"),
            P("sp", None, "tp"),
            P("sp", "tp", None),
        ),
        out_specs=P(("sp", "tp"), None),
        check_vma=False,
    )
```

profile of v0, /device:TPU:17, one launch (start us, length us, event | category | flops | bytes accessed | tf_op | source)
XLA Modules:
  0.0 130.7 jit_solution(7393202836072123514)
XLA Ops:
  0.0 0.9 copy.53
  0.9 0.1 fusion.14
  1.1 0.8 fusion.16
  1.8 0.6 fusion.33
  2.4 0.7 add_convert_fusion.2
  3.1 0.1 broadcast_in_dim.18
  3.2 0.9 copy.55
  4.1 0.8 pad_maximum_fusion.x
  4.9 7.6 %halo.1 = bf16[512,256]{1,0:T(8,128)(2,1)} custom-call(bf16[256,256]{1,0:T(8,128)(2,1)} %pad_maximum_fusion.x), custom_call_target="tpu_custom_call" | custom-call | tf_op jit(solution)/shard_map/halo/pallas_call | solution.py:478
  12.5 1.0 slice_reduce_fusion
  13.6 0.2 fusion.5
  13.8 0.2 multiply_cosine_fusion.1
  14.0 0.1 copy.56
  14.3 1.5 %fusion.2 = (f32[4,256]{1,0:T(4,128)S(1)}, f32[512,256,4]{1,0,2:T(8,128)S(1)}) fusion(pred[256,512]{0,1:T(8,128)(4,1)S(1)} %fusion.5, bf16[256,4,32]{0,2,1:T(8,128)(2,1)S(1)} %get-tuple-element.6, bf16[256,4,32]{0,2,1:T(8,128)(2,1)S(1)} %get-tuple-element.5, bf16[512,256]{1,0:T(8,128)(2,1)} %halo.1), kind=kOutput, calls=%fused_computation.5 | convolution fusion | flops 68942848 | bytes 2494464 | tf_op jit(solution)/shard_map/qhgd,khd->hgqk/dot_general | solution.py:596
  16.0 0.7 convolution_convert_fusion
  16.6 0.8 copy.60.x
  17.4 6.1 %swap.1 = bf16[64,1024]{1,0:T(8,128)(2,1)} custom-call(bf16[256,256]{1,0:T(8,128)(2,1)} %copy.60.x), custom_call_target="tpu_custom_call" | custom-call | tf_op jit(solution)/shard_map/swap/pallas_call | solution.py:534
  23.5 1.0 fusion.7
  24.6 3.3 %multiply_reduce_fusion = (f32[64]{0:T(128)S(1)}, f32[64,2048]{1,0:T(8,128)S(1)}) fusion(bf16[1024,2048]{1,0:T(8,128)(2,1)} %param.25, bf16[64,1024]{1,0:T(8,128)(2,1)} %swap.1, f32[1024]{0:T(1024)S(1)} %copy-done.5, f32[64]{0:T(128)S(1)} %add_rsqrt_fusion.3, bf16[64,2048]{1,0:T(8,128)(2,1)S(1)} %copy-done.2), kind=kOutput, calls=%fused_computation.12 | convolution fusion | flops 269483968 | bytes 5116416 | tf_op jit(solution)/shard_map/dot_general | solution.py:615
  28.0 0.1 multiply_convert_fusion
  28.2 0.1 copy.61
  28.3 0.7 fusion.6.x_in
  29.1 99.7 %moe_exchange.1 = f32[64,2048]{1,0:T(8,128)} custom-call(bf16[64,2176]{1,0:T(8,128)(2,1)} %fusion.6.x_in, bf16[1,2048,512]{2,1,0:T(8,128)(2,1)} %wg_hbm.1, bf16[1,2048,512]{2,1,0:T(8,128)(2,1)} %wu_hbm.1, bf16[1,512,2048]{2,1,0:T(8,128)(2,1)} %wd_hbm.1), custom_call_target="tpu_custom_call" | custom-call | tf_op jit(solution)/shard_map/moe_exchange/pallas_call | solution.py:351
  128.8 1.8 %add_convert_fusion = bf16[64,2048]{1,0:T(8,128)(2,1)} fusion(f32[64,2048]{1,0:T(8,128)S(1)} %get-tuple-element.16, f32[64,2048]{1,0:T(8,128)} %moe_exchange.1), kind=kLoop, calls=%fused_computation.10 | loop fusion | flops 262144 | bytes 1310720 | tf_op jit(solution)/shard_map/convert_element_type | solution.py:632
  (34 shorter events, 0.4 us)
Async XLA Ops:
  0.0 28.1 %copy-start = (s32[256,4]{0,1:T(4,128)S(1)}, s32[256,4]{0,1:T(4,128)}, u32[]{:S(2)}) copy-start(s32[256,4]{0,1:T(4,128)} %param.27) | copy-start | bytes 12292
  0.0 14.0 %copy-start.3 = (bf16[256,256]{1,0:T(8,128)(2,1)S(1)}, bf16[256,256]{1,0:T(8,128)(2,1)}, u32[]{:S(2)}) copy-start(bf16[256,256]{1,0:T(8,128)(2,1)} %param.17) | copy-start | bytes 393220
  0.0 14.2 %copy-start.7 = (f32[64]{0:T(128)S(1)}, f32[64]{0:T(128)}, u32[]{:S(2)}) copy-start(f32[64]{0:T(128)} %param.21) | copy-start | bytes 772
  14.2 1.7 %copy-start.8 = (f32[4]{0:T(128)S(1)}, f32[4]{0:T(128)}, u32[]{:S(2)}) copy-start(f32[4]{0:T(128)} %param.23) | copy-start | bytes 52
  14.2 1.8 %copy-start.1 = (bf16[512,256]{1,0:T(8,128)(2,1)S(1)}, bf16[512,256]{1,0:T(8,128)(2,1)}, u32[]{:S(2)}) copy-start(bf16[512,256]{1,0:T(8,128)(2,1)} %halo.1) | copy-start | bytes 786436
  16.0 8.6 %copy-start.2 = (bf16[64,2048]{1,0:T(8,128)(2,1)S(1)}, bf16[64,2048]{1,0:T(8,128)(2,1)}, u32[]{:S(2)}) copy-start(bf16[64,2048]{1,0:T(8,128)(2,1)} %param.16) | copy-start | bytes 786436
  16.0 8.6 %copy-start.5 = (f32[1024]{0:T(1024)S(1)}, f32[1024]{0:T(1024)}, u32[]{:S(2)}) copy-start(f32[1024]{0:T(1024)} %param.24) | copy-start | bytes 12292
  24.6 3.4 %copy-start.4 = (f32[2048]{0:T(1024)S(1)}, f32[2048]{0:T(1024)}, u32[]{:S(2)}) copy-start(f32[2048]{0:T(1024)} %param.26) | copy-start | bytes 24580
  24.6 3.6 %copy-start.6 = (f32[64,4]{0,1:T(4,128)S(1)}, f32[64,4]{0,1:T(4,128)}, u32[]{:S(2)}) copy-start(f32[64,4]{0,1:T(4,128)} %param.28) | copy-start | bytes 3076
where the time goes:
time: 133 us; the launch traced here: 131 us
  Pallas kernels  114 us (86%)
  other arithmetic  7.4 us (6%)
  matrix products  5.48 us (4%)
  local copies, waits for them, and re-layouts  3.99 us (3%)
    pallas_call x1, Pallas kernels, moe_exchange(): pl.pallas_call(functools.partial(moe_kernel, zn), out_shape=jax.ShapeDtyp...  99.7 us
    pallas_call x1, Pallas kernels, halo(): pl.pallas_call(functools.partial(halo_kernel, lax.axis_size('sp'), width)...  7.62 us
    pallas_call x1, Pallas kernels, swap(): pl.pallas_call(functools.partial(swap_kernel, n), out_shape=jax.ShapeDtyp...  6.14 us
    dot_general x1, matrix products, per_device(): jnp.dot(att_normed, w_out, preferred_element_type=jnp.float32)  3.31 us

commit v1 on v0

--- a/solution.py
+++ b/solution.py
@@ -78,9 +78,9 @@
 
 
 def moe_kernel(
-    zn, x_in, wg_hbm, wu_hbm, wd_hbm, out,
-    X, S, P1, crecv, rx, ry, rdx, rdy, zl, zr, acc, wg, wu, wd,
-    wsem, ag_s, ag_r, c_s, c_r, rs_s, rs_r,
+    zn, x_in, mid, wg_hbm, wu_hbm, wd_hbm, out,
+    X, S, P1, crecv, rx, ry, rdx, rdy, zbuf, acc, wg, wu, wd,
+    wsem, az_s, az_r, ag_s, ag_r, c_s, c_r, rs_s, rs_r, rz_s, rz_r,
 ):
     sp, tp = lax.axis_index("sp"), lax.axis_index("tp")
     z, y = sp // 2, sp % 2
@@ -89,11 +89,15 @@
     D = out.shape[1]
     H = D // 2
     F = wg.shape[1]
-    right, left = (sp + 2, tp), (sp - 2, tp)
     ynb = (z * 2 + (1 - y), tp)
     xnb = (sp, (1 - xx) * 2 + c)
     cnb = (sp, xx * 2 + (1 - c))
-    has_r, has_l = z < zn - 1, z > 0
+
+    def plane(zz):
+        return (zz * 2 + y, tp)
+
+    turn = 2 * (2 * z // zn) - 1
+    far_first = [(z + turn * (1 + k) + 2 * zn) % zn for k in range(zn - 1)] + [z]
 
     loads = [
         pltpu.make_async_copy(src.at[0], dst, wsem.at[i])
@@ -103,19 +107,9 @@
         load.start()
 
     bar = pltpu.get_barrier_semaphore()
-    for nb in (ynb, xnb, cnb):
+    for nb in (ynb, xnb, cnb, *(plane(zz) for zz in far_first[:-1])):
         pl.semaphore_signal(bar, inc=1, device_id=nb, device_id_type=MESH)
-
-    @pl.when(has_r)
-    def _():
-        pl.semaphore_signal(bar, inc=1, device_id=right, device_id_type=MESH)
-
-    @pl.when(has_l)
-    def _():
-        pl.semaphore_signal(bar, inc=1, device_id=left, device_id_type=MESH)
-
-    peers = 3 + (z < zn - 1).astype(jnp.int32) + (z > 0).astype(jnp.int32)
-    pl.semaphore_wait(bar, peers)
+    pl.semaphore_wait(bar, 3 + zn - 1)
 
     def rows(zz):
         return pl.ds(pl.multiple_of(zz * T, T), T)
@@ -129,7 +123,6 @@
 
     def ag(kind, zz, own=False):
         table = {
-            "zr": (0, 0, None, right), "zl": (0, 0, None, left),
             "y": (0, 1, None, ynb), "x": (0, 2, None, xnb),
             "xa": (1, 3, A, xnb), "yb": (2, 3, B, ynb),
             "c0": (0, 4, None, cnb), "c1": (1, 5, None, cnb),
@@ -161,20 +154,16 @@
 
     X[0, rows(z)] = x_in[...]
 
+    def send_plane(zz):
+        return rc(x_in, X.at[0, rows(z)], az_s.at[zz], az_r.at[z], plane(zz))
+
+    def take_plane(zz):
+        return rc(x_in, X.at[0, rows(zz)], az_s.at[zz], az_r.at[zz], plane(zz))
+
     def first(zz, s, side):
         own = s == 0
-        if side == -1:
-            ag("zr", zz).wait_recv()
-        if side == 1:
-            ag("zl", zz).wait_recv()
-        if side <= 0:
-            @pl.when(has_r)
-            def _():
-                ag("zr", zz, own).start()
-        if side >= 0:
-            @pl.when(has_l)
-            def _():
-                ag("zl", zz, own).start()
+        if not own:
+            take_plane(zz).wait_recv()
         for k in ("y", "x", "c0"):
             ag(k, zz, own).start()
 
@@ -229,15 +218,16 @@
             "dyb": (S.at[3, r, hi], rdy.at[r], ynb),
             "ya": (S.at[1, r, lo], ry.at[r, lo], ynb),
             "xb": (S.at[2, r, hi], rx.at[r, hi], xnb),
-            "zr": (S.at[0, r], zl.at[r], right),
-            "zl": (S.at[0, r], zr.at[r], left),
         }
         k = list(table).index(kind)
         src, dst, dev = table[kind]
         return rc(src, dst, rs_s.at[k, zz], rs_r.at[k, zz], dev)
 
-    far = list(range(zn - 1, -1, -1))
+    def sum_plane(zz, source):
+        return rc(S.at[0, rows(zz)], zbuf.at[rows(source)], rz_s.at[zz], rz_r.at[source], plane(zz))
+
     near = list(range(zn))
+    each(lambda zz, s, side: send_plane(zz).start(), near[1:])
 
     for s in range(zn):
         each(first, [s])
@@ -250,23 +240,26 @@
     expert(5)
     group_core(1).start()
     expert(1)
-    each(lambda zz, s, side: rs("yb", zz).start(), far)
+    for zz in far_first:
+        rs("yb", zz).start()
     core_arrivals("c2")
     expert(6)
     group_core(2).start()
     expert(2)
-    each(lambda zz, s, side: rs("xa", zz).start(), far)
+    for zz in far_first:
+        rs("xa", zz).start()
     each(third, near)
     core_arrivals("c3")
     expert(7)
     group_core(3).start()
     expert(3)
 
-    def diag(zz, s, side):
+    def diag(zz):
         rs("dxa", zz).start()
         rs("dyb", zz).start()
 
-    each(diag, far)
+    for zz in far_first[:2]:
+        diag(zz)
     core_arrivals("c0")
     expert(4)
     group_core(0).start()
@@ -274,7 +267,7 @@
 
     f32 = jnp.float32
 
-    def mid_sums(zz, s, side):
+    def mid_sums(zz):
         r = rows(zz)
         rs("dxa", zz).wait_recv()
         S[1, r, lo] = (S[1, r, lo].astype(f32) + rdx[r].astype(f32)).astype(jnp.bfloat16)
@@ -283,63 +276,44 @@
         S[2, r, hi] = (S[2, r, hi].astype(f32) + rdy[r].astype(f32)).astype(jnp.bfloat16)
         rs("xb", zz).start()
 
-    def last_sums(zz, s, side):
+    def last_sums(zz):
         r = rows(zz)
         for k in ("xa", "xb", "ya", "yb"):
             rs(k, zz).wait_recv()
-        acc[...] = S[0, r].astype(f32) + rx[r].astype(f32) + ry[r].astype(f32)
-        if side >= 0:
-            @pl.when(has_l)
-            def _():
-                rs("zr", zz).wait_recv()
-                acc[...] += zl[r].astype(f32)
-        if side <= 0:
-            @pl.when(has_r)
-            def _():
-                rs("zl", zz).wait_recv()
-                acc[...] += zr[r].astype(f32)
-        if s == 0:
-            out[...] = acc[...]
-        else:
-            S[0, r] = acc[...].astype(jnp.bfloat16)
-            if side == 1:
-                rs("zr", zz).start()
-            else:
-                rs("zl", zz).start()
-
-    for i, s in enumerate(far):
-        each(mid_sums, [s])
-        if i > 0:
-            each(last_sums, [far[i - 1]])
-    each(last_sums, [far[-1]])
+        return S[0, r].astype(f32) + rx[r].astype(f32) + ry[r].astype(f32)
+
+    for k, zz in enumerate(far_first):
+        mid_sums(zz)
+        if k + 2 < zn:
+            diag(far_first[k + 2])
+        if k > 0:
+            before = far_first[k - 1]
+            S[0, rows(before)] = last_sums(before).astype(jnp.bfloat16)
+            sum_plane(before, z).start()
+    acc[...] = mid[...].astype(f32) + last_sums(z)
+    for zz in far_first[:-1]:
+        sum_plane(zz, zz).wait_recv()
+        acc[...] += zbuf[rows(zz)].astype(f32)
+    out[...] = acc[...].astype(jnp.bfloat16)
 
     def drain(zz, s, side):
         own = s == 0
-        if side <= 0:
-            @pl.when(has_r)
-            def _():
-                ag("zr", zz, own).wait_send()
-        if side >= 0:
-            @pl.when(has_l)
-            def _():
-                ag("zl", zz, own).wait_send()
         for k in ("y", "x", "c0"):
             ag(k, zz, own).wait_send()
         for k in ("xa", "yb", "c1", "c2", "c3"):
             ag(k, zz).wait_send()
         for k in ("yb", "xa", "dxa", "dyb", "ya", "xb"):
             rs(k, zz).wait_send()
-        if side == 1:
-            rs("zr", zz).wait_send()
-        if side == -1:
-            rs("zl", zz).wait_send()
+        if not own:
+            send_plane(zz).wait_send()
+            sum_plane(zz, z).wait_send()
 
     each(drain, near)
     for q in range(4):
         group_core(q).wait_send()
 
 
-def moe_exchange(x_in, w_gate, w_up, w_down):
+def moe_exchange(x_in, middle, w_gate, w_up, w_down):
     zn = lax.axis_size("sp") // 2
     T, W = x_in.shape
     D = w_gate.shape[1]
@@ -350,8 +324,8 @@
     anyspec = pl.BlockSpec(memory_space=pl.ANY)
     return pl.pallas_call(
         functools.partial(moe_kernel, zn),
-        out_shape=jax.ShapeDtypeStruct((T, D), jnp.float32),
-        in_specs=[vm, anyspec, anyspec, anyspec],
+        out_shape=jax.ShapeDtypeStruct((T, D), bf),
+        in_specs=[vm, vm, anyspec, anyspec, anyspec],
         out_specs=vm,
         scratch_shapes=[
             pltpu.VMEM((8, G, W), bf),
@@ -363,24 +337,27 @@
             pltpu.VMEM((G, D // 2), bf),
             pltpu.VMEM((G, D // 2), bf),
             pltpu.VMEM((G, D), bf),
-            pltpu.VMEM((G, D), bf),
             pltpu.VMEM((T, D), jnp.float32),
             pltpu.VMEM((D, F), bf),
             pltpu.VMEM((D, F), bf),
             pltpu.VMEM((F, D), bf),
             pltpu.SemaphoreType.DMA((3,)),
-            pltpu.SemaphoreType.DMA((10, zn)),
-            pltpu.SemaphoreType.DMA((10, zn)),
+            pltpu.SemaphoreType.DMA((zn,)),
+            pltpu.SemaphoreType.DMA((zn,)),
+            pltpu.SemaphoreType.DMA((8, zn)),
+            pltpu.SemaphoreType.DMA((8, zn)),
             pltpu.SemaphoreType.DMA((4,)),
             pltpu.SemaphoreType.DMA((4,)),
-            pltpu.SemaphoreType.DMA((8, zn)),
-            pltpu.SemaphoreType.DMA((8, zn)),
+            pltpu.SemaphoreType.DMA((6, zn)),
+            pltpu.SemaphoreType.DMA((6, zn)),
+            pltpu.SemaphoreType.DMA((zn,)),
+            pltpu.SemaphoreType.DMA((zn,)),
         ],
         compiler_params=pltpu.CompilerParams(
             collective_id=1, has_side_effects=True, vmem_limit_bytes=VMEM_LIMIT
         ),
         name="moe_exchange",
-    )(x_in, w_gate, w_up, w_down)
+    )(x_in, middle, w_gate, w_up, w_down)
 
 
 def dense_fits(tokens, width, sp_size, tp_size, local_experts, hidden):
@@ -628,8 +605,7 @@
     ):
         tail = row_weights(own_routes, route_weights, expert_count)
         packed = jnp.concatenate([moe_in, tail], axis=1)
-        routed = moe_exchange(packed, w_gate, w_up, w_down)
-        return (middle.astype(jnp.float32) + routed).astype(jnp.bfloat16)
+        return moe_exchange(packed, middle, w_gate, w_up, w_down)
     pair_slot, slot_pair, filled = slot_tables(
         own_routes.reshape(1, quarter * top_count), expert_count, capacity
     )

time: 133 us -> 133 us (level); the launches traced: 131 us -> 133 us
  Pallas kernels: 114 us -> 116 us
  other arithmetic: 7.4 us -> 5.57 us
  local copies, waits for them, and re-layouts: 3.99 us -> 5.66 us
    pallas_call x1, Pallas kernels: 99.7 us -> 102 us  [moe_exchange(): pl.pallas_call(functools.partial(moe_kernel, zn), out_shape=jax.ShapeDtyp...]
    convert_element_type x1 -> x0, other arithmetic: 1.84 us -> none  [per_device(): return (middle.astype(jnp.float32) + routed).astype(jnp.bfloat16)]
    unnamed x20 -> x23, local copies, waits for them, and re-layouts: 1.82 us -> 3.5 us
where the time goes in v1:
time: 133 us
  Pallas kernels  116 us (87%)
  local copies, waits for them, and re-layouts  5.66 us (4%)
  other arithmetic  5.57 us (4%)
  matrix products  5.5 us (4%)
    pallas_call x1, Pallas kernels, moe_exchange(): pl.pallas_call(functools.partial(moe_kernel, zn), out_shape=jax.ShapeDtyp...  102 us
    pallas_call x1, Pallas kernels, halo(): pl.pallas_call(functools.partial(halo_kernel, lax.axis_size('sp'), width)...  7.62 us
    pallas_call x1, Pallas kernels, swap(): pl.pallas_call(functools.partial(swap_kernel, n), out_shape=jax.ShapeDtyp...  6.14 us
    unnamed x23, local copies, waits for them, and re-layouts  3.5 us
    dot_general x1, matrix products, per_device(): jnp.dot(att_normed, w_out, preferred_element_type=jnp.float32)  3.33 us

profile of v1, /device:TPU:17, one launch (start us, length us, event | category | flops | bytes accessed | tf_op | source)
XLA Modules:
  0.0 132.9 jit_solution(8474011307611418227)
XLA Ops:
  0.0 0.9 copy.53
  0.9 0.1 fusion.16
  1.1 0.8 fusion.18
  1.8 0.6 fusion.35
  2.4 0.7 add_convert_fusion.1
  3.1 0.1 broadcast_in_dim.18
  3.2 0.9 copy.55
  4.1 0.8 pad_maximum_fusion.x
  4.9 7.6 %halo.1 = bf16[512,256]{1,0:T(8,128)(2,1)} custom-call(bf16[256,256]{1,0:T(8,128)(2,1)} %pad_maximum_fusion.x), custom_call_target="tpu_custom_call" | custom-call | tf_op jit(solution)/shard_map/halo/pallas_call | solution.py:455
  12.5 1.0 slice_reduce_fusion
  13.6 0.2 fusion.7
  13.8 0.2 multiply_cosine_fusion.1
  14.0 0.1 copy.56
  14.3 1.5 %fusion.1 = (f32[4,256]{1,0:T(4,128)S(1)}, f32[512,256,4]{1,0,2:T(8,128)S(1)}) fusion(pred[256,512]{0,1:T(8,128)(4,1)S(1)} %fusion.7, bf16[256,4,32]{0,2,1:T(8,128)(2,1)S(1)} %get-tuple-element.6, bf16[256,4,32]{0,2,1:T(8,128)(2,1)S(1)} %get-tuple-element.5, bf16[512,256]{1,0:T(8,128)(2,1)} %halo.1), kind=kOutput, calls=%fused_computation.4 | convolution fusion | flops 68942848 | bytes 2494464 | tf_op jit(solution)/shard_map/qhgd,khd->hgqk/dot_general | solution.py:573
  16.0 0.7 convolution_convert_fusion
  16.6 0.8 copy.60.x
  17.4 6.1 %swap.1 = bf16[64,1024]{1,0:T(8,128)(2,1)} custom-call(bf16[256,256]{1,0:T(8,128)(2,1)} %copy.60.x), custom_call_target="tpu_custom_call" | custom-call | tf_op jit(solution)/shard_map/swap/pallas_call | solution.py:511
  23.5 1.0 fusion.9
  24.6 3.3 %fusion.4 = (f32[64]{0:T(128)S(1)}, bf16[64,2048]{1,0:T(8,128)(2,1)S(1)}) fusion(bf16[1024,2048]{1,0:T(8,128)(2,1)} %param.25, bf16[64,1024]{1,0:T(8,128)(2,1)} %swap.1, f32[1024]{0:T(1024)S(1)} %copy-done.6, f32[64]{0:T(128)S(1)} %add_rsqrt_fusion.3, bf16[64,2048]{1,0:T(8,128)(2,1)S(1)} %copy-done.3), kind=kOutput, calls=%fused_computation.11 | convolution fusion | flops 269483968 | bytes 4854272 | tf_op jit(solution)/shard_map/dot_general | solution.py:592
  28.0 0.1 fusion.6
  28.3 0.1 copy.61
  28.4 0.7 fusion.8.x_in
  29.1 102.1 %moe_exchange.1 = bf16[64,2048]{1,0:T(8,128)(2,1)} custom-call(bf16[64,2176]{1,0:T(8,128)(2,1)} %fusion.8.x_in, bf16[64,2048]{1,0:T(8,128)(2,1)} %copy-done.1, bf16[1,2048,512]{2,1,0:T(8,128)(2,1)} %wg_hbm.1, bf16[1,2048,512]{2,1,0:T(8,128)(2,1)} %wu_hbm.1, bf16[1,512,2048]{2,1,0:T(8,128)(2,1)} %wd_hbm.1), custom_call_target="tpu_custom_call" | custom-call | tf_op jit(solution)/shard_map/moe_exchange/pallas_call | solution.py:325
  131.3 1.7 %copy.68 = bf16[64,2048]{1,0:T(8,128)(2,1)} copy(bf16[64,2048]{1,0:T(8,128)(2,1)} %moe_exchange.1) | data formatting | bytes 524288
  (36 shorter events, 0.4 us)
Async XLA Ops:
  0.0 28.1 %copy-start = (s32[256,4]{0,1:T(4,128)S(1)}, s32[256,4]{0,1:T(4,128)}, u32[]{:S(2)}) copy-start(s32[256,4]{0,1:T(4,128)} %param.27) | copy-start | bytes 12292
  0.0 14.0 %copy-start.4 = (bf16[256,256]{1,0:T(8,128)(2,1)S(1)}, bf16[256,256]{1,0:T(8,128)(2,1)}, u32[]{:S(2)}) copy-start(bf16[256,256]{1,0:T(8,128)(2,1)} %param.17) | copy-start | bytes 393220
  0.0 14.2 %copy-start.8 = (f32[64]{0:T(128)S(1)}, f32[64]{0:T(128)}, u32[]{:S(2)}) copy-start(f32[64]{0:T(128)} %param.21) | copy-start | bytes 772
  14.2 1.7 %copy-start.9 = (f32[4]{0:T(128)S(1)}, f32[4]{0:T(128)}, u32[]{:S(2)}) copy-start(f32[4]{0:T(128)} %param.23) | copy-start | bytes 52
  14.2 1.8 %copy-start.2 = (bf16[512,256]{1,0:T(8,128)(2,1)S(1)}, bf16[512,256]{1,0:T(8,128)(2,1)}, u32[]{:S(2)}) copy-start(bf16[512,256]{1,0:T(8,128)(2,1)} %halo.1) | copy-start | bytes 786436
  16.0 8.6 %copy-start.3 = (bf16[64,2048]{1,0:T(8,128)(2,1)S(1)}, bf16[64,2048]{1,0:T(8,128)(2,1)}, u32[]{:S(2)}) copy-start(bf16[64,2048]{1,0:T(8,128)(2,1)} %param.16) | copy-start | bytes 786436
  16.0 8.6 %copy-start.6 = (f32[1024]{0:T(1024)S(1)}, f32[1024]{0:T(1024)}, u32[]{:S(2)}) copy-start(f32[1024]{0:T(1024)} %param.24) | copy-start | bytes 12292
  24.6 3.4 %copy-start.5 = (f32[2048]{0:T(1024)S(1)}, f32[2048]{0:T(1024)}, u32[]{:S(2)}) copy-start(f32[2048]{0:T(1024)} %param.26) | copy-start | bytes 24580
  24.6 3.6 %copy-start.7 = (f32[64,4]{0,1:T(4,128)S(1)}, f32[64,4]{0,1:T(4,128)}, u32[]{:S(2)}) copy-start(f32[64,4]{0,1:T(4,128)} %param.28) | copy-start | bytes 3076
  28.0 1.1 copy-start.1

commit v2 on v1

--- a/solution.py
+++ b/solution.py
@@ -7,33 +7,10 @@
 from jax.experimental.pallas import tpu as pltpu
 from jax.sharding import PartitionSpec as P
 
-WINDOW = 128
-
-
 rope_base = 10000.0
 norm_eps = 1e-06
 swiglu_limit = 7.0
 swiglu_alpha = 1.702
-
-
-def row_normalize(values, gain_vec):
-    floats = values.astype(jnp.float32)
-    scale_inv = lax.rsqrt(jnp.mean(floats * floats, axis=-1, keepdims=True) + norm_eps)
-    return floats * scale_inv * gain_vec
-
-
-def apply_rotary_heads(heads, token_positions):
-    half_size = heads.shape[-1] // 2
-    freqs = rope_base ** (-jnp.arange(half_size, dtype=jnp.float32) / half_size)
-    angles = token_positions[:, None] * freqs[None, :]
-    cosine = jnp.cos(angles)[:, None, :]
-    sine = jnp.sin(angles)[:, None, :]
-    first_half = heads[..., :half_size]
-    second_half = heads[..., half_size:]
-    return jnp.concatenate(
-        [first_half * cosine - second_half * sine, first_half * sine + second_half * cosine],
-        axis=-1,
-    )
 
 
 def expert_act(gate_pre, up_pre):
@@ -80,7 +57,7 @@
 def moe_kernel(
     zn, x_in, mid, wg_hbm, wu_hbm, wd_hbm, out,
     X, S, P1, crecv, rx, ry, rdx, rdy, zbuf, acc, wg, wu, wd,
-    wsem, az_s, az_r, ag_s, ag_r, c_s, c_r, rs_s, rs_r, rz_s, rz_r,
+    wsem, ag_s, ag_r, c_s, c_r, rs_s, rs_r, rz_s, rz_r,
 ):
     sp, tp = lax.axis_index("sp"), lax.axis_index("tp")
     z, y = sp // 2, sp % 2
@@ -96,6 +73,9 @@
     def plane(zz):
         return (zz * 2 + y, tp)
 
+    right, left = plane(z + 1), plane(z - 1)
+    has_r, has_l = z < zn - 1, z > 0
+
     turn = 2 * (2 * z // zn) - 1
     far_first = [(z + turn * (1 + k) + 2 * zn) % zn for k in range(zn - 1)] + [z]
 
@@ -123,6 +103,7 @@
 
     def ag(kind, zz, own=False):
         table = {
+            "zr": (0, 0, None, right), "zl": (0, 0, None, left),
             "y": (0, 1, None, ynb), "x": (0, 2, None, xnb),
             "xa": (1, 3, A, xnb), "yb": (2, 3, B, ynb),
             "c0": (0, 4, None, cnb), "c1": (1, 5, None, cnb),
@@ -154,16 +135,20 @@
 
     X[0, rows(z)] = x_in[...]
 
-    def send_plane(zz):
-        return rc(x_in, X.at[0, rows(z)], az_s.at[zz], az_r.at[z], plane(zz))
-
-    def take_plane(zz):
-        return rc(x_in, X.at[0, rows(zz)], az_s.at[zz], az_r.at[zz], plane(zz))
-
     def first(zz, s, side):
         own = s == 0
-        if not own:
-            take_plane(zz).wait_recv()
+        if side == -1:
+            ag("zr", zz).wait_recv()
+        if side == 1:
+            ag("zl", zz).wait_recv()
+        if side <= 0:
+            @pl.when(has_r)
+            def _():
+                ag("zr", zz, own).start()
+        if side >= 0:
+            @pl.when(has_l)
+            def _():
+                ag("zl", zz, own).start()
         for k in ("y", "x", "c0"):
             ag(k, zz, own).start()
 
@@ -227,7 +212,6 @@
         return rc(S.at[0, rows(zz)], zbuf.at[rows(source)], rz_s.at[zz], rz_r.at[source], plane(zz))
 
     near = list(range(zn))
-    each(lambda zz, s, side: send_plane(zz).start(), near[1:])
 
     for s in range(zn):
         each(first, [s])
@@ -298,6 +282,14 @@
 
     def drain(zz, s, side):
         own = s == 0
+        if side <= 0:
+            @pl.when(has_r)
+            def _():
+                ag("zr", zz, own).wait_send()
+        if side >= 0:
+            @pl.when(has_l)
+            def _():
+                ag("zl", zz, own).wait_send()
         for k in ("y", "x", "c0"):
             ag(k, zz, own).wait_send()
         for k in ("xa", "yb", "c1", "c2", "c3"):
@@ -305,7 +297,6 @@
         for k in ("yb", "xa", "dxa", "dyb", "ya", "xb"):
             rs(k, zz).wait_send()
         if not own:
-            send_plane(zz).wait_send()
             sum_plane(zz, z).wait_send()
 
     each(drain, near)
@@ -342,10 +333,8 @@
             pltpu.VMEM((D, F), bf),
             pltpu.VMEM((F, D), bf),
             pltpu.SemaphoreType.DMA((3,)),
-            pltpu.SemaphoreType.DMA((zn,)),
-            pltpu.SemaphoreType.DMA((zn,)),
-            pltpu.SemaphoreType.DMA((8, zn)),
-            pltpu.SemaphoreType.DMA((8, zn)),
+            pltpu.SemaphoreType.DMA((10, zn)),
+            pltpu.SemaphoreType.DMA((10, zn)),
             pltpu.SemaphoreType.DMA((4,)),
             pltpu.SemaphoreType.DMA((4,)),
             pltpu.SemaphoreType.DMA((6, zn)),
@@ -385,142 +374,213 @@
     return jnp.pad(both, ((0, 0), (0, LANES - 2 * expert_count)))
 
 
-def halo_kernel(peers, width, x, out, before, after, ss, rs):
-    sp, tp = lax.axis_index("sp"), lax.axis_index("tp")
-    length = x.shape[0]
-    up, down = (sp + 1, tp), (sp - 1, tp)
+def front_kernel(
+    peers, n, q_in, k_in, v_in, docs_row, angle_in, q_gain, k_gain, sink,
+    out_gain, resid, norm_gain, tail, w_hbm, mid, packed,
+    kv, span, att, held, w, wsem, kv_s, kv_r, doc_s, doc_r, ss, rs,
+):
+    sp, me = lax.axis_index("sp"), lax.axis_index("tp")
+    f32, bf = jnp.float32, jnp.bfloat16
+    head, length = k_in.shape
+    width = LANES
+    half = head // 2
+    heads = q_in.shape[1] // head
+    blocks = length // width
+    part_rows = length // n
+    D = mid.shape[1]
+    up, down = (sp + 1, me), (sp - 1, me)
     has_up, has_down = sp < peers - 1, sp > 0
-    bar = pltpu.get_barrier_semaphore()
-
-    def send(part, dst, i, dev):
-        return pltpu.make_async_remote_copy(
-            src_ref=part, dst_ref=dst, send_sem=ss.at[i], recv_sem=rs.at[i],
-            device_id=dev, device_id_type=MESH,
-        )
-
-    go_up = send(x.at[pl.ds(length - width, width)], before, 0, up)
-    go_down = send(x.at[pl.ds(0, width)], after, 1, down)
-
-    @pl.when(has_up)
-    def _():
-        pl.semaphore_signal(bar, inc=1, device_id=up, device_id_type=MESH)
-
-    @pl.when(has_down)
-    def _():
-        pl.semaphore_signal(bar, inc=1, device_id=down, device_id_type=MESH)
-
-    pl.semaphore_wait(bar, has_up.astype(jnp.int32) + has_down.astype(jnp.int32))
-
-    @pl.when(has_up)
-    def _():
-        go_up.start()
-
-    @pl.when(has_down)
-    def _():
-        go_down.start()
-
-    out[pl.ds(width, length)] = x[...]
-    edge = jnp.zeros(before.shape, before.dtype)
-
-    @pl.when(has_down)
-    def _():
-        go_up.wait_recv()
-        out[pl.ds(0, width)] = before[...]
-
-    @pl.when(jnp.logical_not(has_down))
-    def _():
-        out[pl.ds(0, width)] = edge
-
-    @pl.when(has_up)
-    def _():
-        go_down.wait_recv()
-        out[pl.ds(length + width, width)] = after[...]
-
-    @pl.when(jnp.logical_not(has_up))
-    def _():
-        out[pl.ds(length + width, width)] = edge
-
-    @pl.when(has_up)
-    def _():
-        go_up.wait_send()
-
-    @pl.when(has_down)
-    def _():
-        go_down.wait_send()
-
-
-def halo(x, width):
-    length, columns = x.shape
-    vm = pl.BlockSpec(memory_space=pltpu.VMEM)
-    return pl.pallas_call(
-        functools.partial(halo_kernel, lax.axis_size("sp"), width),
-        out_shape=jax.ShapeDtypeStruct((length + 2 * width, columns), x.dtype),
-        in_specs=[vm],
-        out_specs=vm,
-        scratch_shapes=[
-            pltpu.VMEM((width, columns), x.dtype),
-            pltpu.VMEM((width, columns), x.dtype),
-            pltpu.SemaphoreType.DMA((2,)),
-            pltpu.SemaphoreType.DMA((2,)),
-        ],
-        compiler_params=pltpu.CompilerParams(collective_id=2, has_side_effects=True),
-        name="halo",
-    )(x)
-
-
-def swap_kernel(n, x, out, held, ss, rs):
-    sp, me = lax.axis_index("sp"), lax.axis_index("tp")
-    q, columns = out.shape[0], x.shape[1]
+    load = pltpu.make_async_copy(w_hbm, w, wsem.at[0])
+    load.start()
+
     bar = pltpu.get_barrier_semaphore()
     for p in range(1, n):
         pl.semaphore_signal(bar, inc=1, device_id=(sp, (me + p) % n), device_id_type=MESH)
-    pl.semaphore_wait(bar, n - 1)
-
-    def send(p):
+
+    @pl.when(has_up)
+    def _():
+        pl.semaphore_signal(bar, inc=1, device_id=up, device_id_type=MESH)
+
+    @pl.when(has_down)
+    def _():
+        pl.semaphore_signal(bar, inc=1, device_id=down, device_id_type=MESH)
+
+    def rc(src, dst, send_sem, recv_sem, dev):
+        return pltpu.make_async_remote_copy(
+            src_ref=src, dst_ref=dst, send_sem=send_sem, recv_sem=recv_sem,
+            device_id=dev, device_id_type=MESH,
+        )
+
+    go_up = (
+        rc(kv.at[pl.ds(length, width)], kv.at[pl.ds(0, width)], kv_s.at[0], kv_r.at[0], up),
+        rc(docs_row.at[blocks - 1], span.at[0], doc_s.at[0], doc_r.at[0], up),
+    )
+    go_down = (
+        rc(kv.at[pl.ds(width, width)], kv.at[pl.ds(length + width, width)], kv_s.at[1], kv_r.at[1], down),
+        rc(docs_row.at[0], span.at[blocks + 1], doc_s.at[1], doc_r.at[1], down),
+    )
+    table = jnp.transpose(jnp.concatenate([angle_in[...]] * 2, axis=0))
+    cosine, sine = table[:, :half], table[:, half:head]
+    own = jnp.concatenate([k_in[...].astype(f32), v_in[...].astype(f32)], axis=0)
+    own = jnp.transpose(own)
+
+    def rotated(x, gain):
+        x = x * lax.rsqrt(jnp.mean(x * x, axis=1, keepdims=True) + norm_eps) * gain
+        a, b = x[:, :half], x[:, half:]
+        return jnp.concatenate([a * cosine - b * sine, a * sine + b * cosine], axis=1).astype(bf)
+
+    kv[pl.ds(width, length)] = jnp.concatenate(
+        [rotated(own[:, :head], k_gain[...]), own[:, head:].astype(bf)], axis=1
+    )
+    pl.semaphore_wait(bar, n - 1 + has_up.astype(jnp.int32) + has_down.astype(jnp.int32))
+
+    @pl.when(has_up)
+    def _():
+        for copy in go_up:
+            copy.start()
+
+    @pl.when(has_down)
+    def _():
+        for copy in go_down:
+            copy.start()
+
+    span[pl.ds(1, blocks)] = docs_row[...]
+
+    @pl.when(jnp.logical_not(has_down))
+    def _():
+        kv[pl.ds(0, width)] = jnp.zeros((width, 2 * head), bf)
+        span[0] = jnp.full((1, width), -1, jnp.int32)
+
+    @pl.when(jnp.logical_not(has_up))
+    def _():
+        kv[pl.ds(length + width, width)] = jnp.zeros((width, 2 * head), bf)
+        span[blocks + 1] = jnp.full((1, width), -1, jnp.int32)
+
+    queries = q_in[...].astype(f32)
+    q_rot = [rotated(queries[:, h * head : (h + 1) * head], q_gain[...]) for h in range(heads)]
+
+    @pl.when(has_down)
+    def _():
+        for copy in go_up:
+            copy.wait_recv()
+
+    @pl.when(has_up)
+    def _():
+        for copy in go_down:
+            copy.wait_recv()
+
+    row = lax.broadcasted_iota(jnp.int32, (width, width), 0)
+    col = lax.broadcasted_iota(jnp.int32, (width, width), 1)
+    for b in range(blocks):
+        own_doc = jnp.broadcast_to(docs_row[b].astype(f32), (width, width))
+        own_doc = jnp.transpose(own_doc)
+        same = [own_doc == span[b + j].astype(f32) for j in range(3)]
+        allowed = jnp.concatenate([same[0] & (col >= row), same[1], same[2] & (col <= row)], axis=1)
+        both = kv[pl.ds(b * width, 3 * width)]
+        key_rows, value_rows = both[:, :head], both[:, head:]
+        mixed = []
+        for h in range(heads):
+            scores = lax.dot_general(
+                q_rot[h][b * width : (b + 1) * width], key_rows, (((1,), (1,)), ((), ())),
+                preferred_element_type=f32,
+            )
+            raw = jnp.where(allowed, jnp.exp(scores * head**-0.5), 0.0)
+            total = jnp.sum(raw, axis=1, keepdims=True) + jnp.exp(jnp.full((1, 1), sink[h]))
+            probs = (raw / total).astype(bf)
+            mixed.append(jnp.dot(probs, value_rows, preferred_element_type=f32))
+        att[pl.ds(b * width, width)] = jnp.concatenate(mixed, axis=1).astype(bf)
+
+    def own_part(to):
+        return pl.ds(pl.multiple_of(to * part_rows, part_rows), part_rows)
+
+    def swap(p):
         to = (me + p) % n
-        part = pl.ds(pl.multiple_of(to * q, q), q)
-        return pltpu.make_async_remote_copy(
-            src_ref=x.at[part], dst_ref=held.at[me], send_sem=ss.at[p], recv_sem=rs.at[me],
-            device_id=(sp, to), device_id_type=MESH,
-        )
+        return rc(att.at[own_part(to)], held.at[me], ss.at[p], rs.at[me], (sp, to))
+
+    def arrival(p):
+        source = (me + p) % n
+        return rc(held.at[source], held.at[source], ss.at[0], rs.at[source], (sp, source))
 
     for p in range(1, n):
-        send(p).start()
-    for s in range(n):
-        cols = pl.ds(s * columns, columns)
-
-        @pl.when(me == s)
-        def _(cols=cols):
-            out[:, cols] = x[pl.ds(pl.multiple_of(me * q, q), q)]
-
-        @pl.when(me != s)
-        def _(cols=cols, s=s):
-            pltpu.make_async_remote_copy(
-                src_ref=held.at[s], dst_ref=held.at[s], send_sem=ss.at[0], recv_sem=rs.at[s],
-                device_id=(sp, (me + 1) % n), device_id_type=MESH,
-            ).wait_recv()
-            out[:, cols] = held[s]
+        swap(p).start()
+    held[me] = att[own_part(me)]
     for p in range(1, n):
-        send(p).wait_send()
-
-
-def swap(x):
+        arrival(p).wait_recv()
+    by_token = jnp.concatenate([held[s] for s in range(n)], axis=1).astype(f32)
+    inverse = lax.rsqrt(jnp.mean(by_token * by_token, axis=1, keepdims=True) + norm_eps)
+    att_normed = (by_token * inverse * out_gain[...]).astype(bf)
+    load.wait()
+    step = D // 4
+    squares = jnp.zeros((part_rows, 1), f32)
+    for c in range(0, D, step):
+        cols = pl.ds(c, step)
+        value = jnp.dot(att_normed, w[:, cols], preferred_element_type=f32)
+        value = (resid[:, cols].astype(f32) + value).astype(bf)
+        mid[:, cols] = value
+        value = value.astype(f32)
+        squares = squares + jnp.sum(value * value, axis=1, keepdims=True)
+    inverse = lax.rsqrt(squares / D + norm_eps)
+    for c in range(0, D, step):
+        cols = pl.ds(c, step)
+        packed[:, cols] = (mid[:, cols].astype(f32) * inverse * norm_gain[:, cols]).astype(bf)
+    packed[:, pl.ds(D, LANES)] = tail[...]
+
+    @pl.when(has_up)
+    def _():
+        for copy in go_up:
+            copy.wait_send()
+
+    @pl.when(has_down)
+    def _():
+        for copy in go_down:
+            copy.wait_send()
+
+    for p in range(1, n):
+        swap(p).wait_send()
+
+
+def front(
+    queries, keys, values, docs, angle_table, q_gain, key_norm_gain, sink,
+    out_gain, resid, norm_gain, tail, w_out,
+):
     n = lax.axis_size("tp")
-    length, columns = x.shape
+    length, head = keys.shape
+    columns = queries.shape[1]
+    rows, D = resid.shape
+    bf = jnp.bfloat16
+    blocks = length // LANES
     vm = pl.BlockSpec(memory_space=pltpu.VMEM)
+    smem = pl.BlockSpec(memory_space=pltpu.SMEM)
     return pl.pallas_call(
-        functools.partial(swap_kernel, n),
-        out_shape=jax.ShapeDtypeStruct((length // n, n * columns), x.dtype),
-        in_specs=[vm],
-        out_specs=vm,
+        functools.partial(front_kernel, lax.axis_size("sp"), n),
+        out_shape=(
+            jax.ShapeDtypeStruct((rows, D), bf),
+            jax.ShapeDtypeStruct((rows, D + LANES), bf),
+        ),
+        in_specs=[vm] * 7 + [smem] + [vm] * 4 + [pl.BlockSpec(memory_space=pl.ANY)],
+        out_specs=(vm, vm),
         scratch_shapes=[
-            pltpu.VMEM((n, length // n, columns), x.dtype),
+            pltpu.VMEM((length + 2 * LANES, 2 * head), bf),
+            pltpu.VMEM((blocks + 2, 1, LANES), jnp.int32),
+            pltpu.VMEM((length, columns), bf),
+            pltpu.VMEM((n, rows, columns), bf),
+            pltpu.VMEM(w_out.shape, bf),
+            pltpu.SemaphoreType.DMA((1,)),
+            pltpu.SemaphoreType.DMA((2,)),
+            pltpu.SemaphoreType.DMA((2,)),
+            pltpu.SemaphoreType.DMA((2,)),
+            pltpu.SemaphoreType.DMA((2,)),
             pltpu.SemaphoreType.DMA((n,)),
             pltpu.SemaphoreType.DMA((n,)),
         ],
-        compiler_params=pltpu.CompilerParams(collective_id=3, has_side_effects=True),
-        name="swap",
-    )(x)
+        compiler_params=pltpu.CompilerParams(
+            collective_id=2, has_side_effects=True, vmem_limit_bytes=VMEM_LIMIT
+        ),
+        name="front",
+    )(
+        queries, keys.T, values.T, docs.reshape(blocks, 1, LANES), angle_table,
+        q_gain[None], key_norm_gain[None], sink, out_gain[None], resid, norm_gain[None], tail, w_out,
+    )
 
 
 def per_device(
@@ -546,66 +606,35 @@
     sp_index = lax.axis_index("sp")
     tp_index = lax.axis_index("tp")
     tok_rows = queries.shape[0]
-    head_size = q_gain.shape[0]
-    query_heads = sink.shape[0]
-    kv_heads = keys.shape[1] // head_size
-    query_group_width = query_heads // kv_heads
+    half_size = q_gain.shape[0] // 2
     token_positions = (sp_index * tok_rows + jnp.arange(tok_rows, dtype=jnp.int32)).astype(
         jnp.float32
     )
-    q_rot = apply_rotary_heads(
-        row_normalize(queries.reshape(tok_rows, query_heads, head_size), q_gain), token_positions
-    ).astype(jnp.bfloat16)
-    key_rotated = apply_rotary_heads(
-        row_normalize(keys.reshape(tok_rows, kv_heads, head_size), key_norm_gain), token_positions
-    ).astype(jnp.bfloat16)
-    key_value = jnp.concatenate(
-        [key_rotated.reshape(tok_rows, kv_heads * head_size), values], axis=1
-    )
-    doc_mark = (docs + 1).astype(jnp.bfloat16)
-    kv_width = key_value.shape[1]
-    marks = jnp.broadcast_to(doc_mark[:, None], (tok_rows, LANES))
-    packed_span = halo(jnp.concatenate([key_value, marks], axis=1), WINDOW)
-    kv_span, doc_span = packed_span[:, :kv_width], packed_span[:, kv_width]
-    span_rows = tok_rows + 2 * WINDOW
-    k_span = kv_span[:, : kv_heads * head_size].reshape(span_rows, kv_heads, head_size)
-    v_span = kv_span[:, kv_heads * head_size :].reshape(span_rows, kv_heads, head_size)
-    scores = jnp.einsum(
-        "qhgd,khd->hgqk",
-        q_rot.reshape(tok_rows, kv_heads, query_group_width, head_size),
-        k_span,
-        preferred_element_type=jnp.float32,
-    ) * head_size ** (-0.5)
-    offsets = jnp.arange(tok_rows, dtype=jnp.int32)[:, None] - (
-        jnp.arange(span_rows, dtype=jnp.int32)[None, :] - WINDOW
-    )
-    allowed = (jnp.abs(offsets) <= WINDOW) & (doc_mark[:, None] == doc_span[None, :])
-    raw_weights = jnp.where(allowed[None, None], jnp.exp(scores), jnp.zeros((), jnp.float32))
-    sink_exponent = jnp.exp(sink).reshape(kv_heads, query_group_width)
-    total = jnp.sum(raw_weights, axis=-1) + sink_exponent[:, :, None]
-    probs = (raw_weights / total[..., None]).astype(jnp.bfloat16)
-    att = jnp.einsum("hgqk,khd->qhgd", probs, v_span, preferred_element_type=jnp.float32)
-    att = att.astype(jnp.bfloat16).reshape(tok_rows, query_heads * head_size)
-    by_token = swap(att)
-    att_normed = row_normalize(by_token, out_gain).astype(jnp.bfloat16)
-    middle = (
-        resid.astype(jnp.float32) + jnp.dot(att_normed, w_out, preferred_element_type=jnp.float32)
-    ).astype(jnp.bfloat16)
-    moe_in = row_normalize(middle, norm_gain).astype(jnp.bfloat16)
+    freqs = rope_base ** (-jnp.arange(half_size, dtype=jnp.float32) / half_size)
+    angles = freqs[:, None] * token_positions[None, :]
+    angle_table = jnp.concatenate([jnp.cos(angles), jnp.sin(angles)], axis=0)
     quarter = tok_rows // tp_size
     top_count = routes.shape[1]
     local_experts = w_gate.shape[0]
     expert_count = sp_size * local_experts
     capacity = 3 * quarter * top_count // (2 * expert_count) + 2
-    model_width = moe_in.shape[1]
+    model_width = resid.shape[1]
     empty = jnp.zeros((), jnp.bfloat16)
     own_routes = lax.dynamic_slice_in_dim(routes, tp_index * quarter, quarter, 0)
-    if dense_fits(
+    dense = dense_fits(
         tok_rows * sp_size, model_width, sp_size, tp_size, local_experts, w_gate.shape[2]
-    ):
+    )
+    if dense:
         tail = row_weights(own_routes, route_weights, expert_count)
-        packed = jnp.concatenate([moe_in, tail], axis=1)
+    else:
+        tail = jnp.zeros((quarter, LANES), jnp.bfloat16)
+    middle, packed = front(
+        queries, keys, values, docs, angle_table, q_gain, key_norm_gain, sink,
+        out_gain, resid, norm_gain, tail, w_out,
+    )
+    if dense:
         return moe_exchange(packed, middle, w_gate, w_up, w_down)
+    moe_in = packed[:, :model_width]
     pair_slot, slot_pair, filled = slot_tables(
         own_routes.reshape(1, quarter * top_count), expert_count, capacity
     )

time: 133 us -> 117 us (0.88); the launches traced: 133 us -> 116 us
  matrix products: 5.5 us -> 0 us
  Pallas kernels: 116 us -> 111 us
  other arithmetic: 5.57 us -> 1.56 us
  local copies, waits for them, and re-layouts: 5.66 us -> 3.12 us
    pallas_call x1, Pallas kernels: 102 us -> 96.2 us  [moe_exchange(): pl.pallas_call(functools.partial(moe_kernel, zn), out_shape=jax.ShapeDtyp...]
    dot_general x3 -> x0, matrix products: 5.5 us -> none  [the longest x1 3.33 us: per_device(): jnp.dot(att_normed, w_out, preferred_element_type=jnp.float32)]
    concatenate x3 -> x1, other arithmetic: 2.11 us -> 0.64 us  [per_device(): angle_table = jnp.concatenate([jnp.cos(angles), jnp.sin(angles)], axis=0)]
    unnamed x23 -> x3, local copies, waits for them, and re-layouts: 3.5 us -> 2.34 us
    pallas_call x2 -> x1, Pallas kernels: 13.8 us -> 14.6 us  [front(): pl.pallas_call(functools.partial(front_kernel, lax.axis_size('sp'), n), o...]
where the time goes in v2:
time: 117 us; the launch traced here: 116 us
  Pallas kernels  111 us (95%)
  local copies, waits for them, and re-layouts  3.12 us (3%)
  other arithmetic  1.56 us (1%)
    pallas_call x1, Pallas kernels, moe_exchange(): pl.pallas_call(functools.partial(moe_kernel, zn), out_shape=jax.ShapeDtyp...  96.2 us
    pallas_call x1, Pallas kernels, front(): pl.pallas_call(functools.partial(front_kernel, lax.axis_size('sp'), n), o...  14.6 us

profile of v2, /device:TPU:17, one launch (start us, length us, event | category | flops | bytes accessed | tf_op | source)
XLA Modules:
  0.0 115.6 jit_solution(13498681652984488251)
XLA Ops:
  0.0 0.0 copy-start
  0.0 0.7 copy-done
  0.7 0.1 constant_dynamic-slice_fusion
  0.8 0.7 select_reduce_fusion
  1.5 0.1 copy.22
  1.6 0.6 pad.4.tail
  2.2 0.2 multiply_cosine_fusion
  2.4 0.6 pad_maximum_fusion.angle_in
  3.0 14.6 %front.1 = (bf16[64,2048]{1,0:T(8,128)(2,1)}, bf16[64,2176]{1,0:T(8,128)(2,1)}) custom-call(bf16[256,256]{1,0:T(8,128)(2,1)} %q_in.1, bf16[64,256]{1,0:T(8,128)(2,1)} %bitcast.7, bf16[64,256]{1,0:T(8,128)(2,1)} %bitcast.8, s32[2,1,128]{2,1,0:T(1,128)} %bitcast.11, f32[64,256]{1,0:T(8,128)} %pad_maximum_fusion.angle_in, f32[1,64]{1,0:T(1,128)} %bitcast.12, ...), custom_call_target="tpu_custom_call" | custom-call | tf_op jit(solution)/shard_map/front/pallas_call | solution.py:554
  17.7 96.2 %moe_exchange.1 = bf16[64,2048]{1,0:T(8,128)(2,1)} custom-call(bf16[64,2176]{1,0:T(8,128)(2,1)} %get-tuple-element.7.x_in, bf16[64,2048]{1,0:T(8,128)(2,1)} %get-tuple-element.8.mid, bf16[1,2048,512]{2,1,0:T(8,128)(2,1)} %wg_hbm.1, bf16[1,2048,512]{2,1,0:T(8,128)(2,1)} %wu_hbm.1, bf16[1,512,2048]{2,1,0:T(8,128)(2,1)} %wd_hbm.1), custom_call_target="tpu_custom_call" | custom-call | tf_op jit(solution)/shard_map/moe_exchange/pallas_call | solution.py:316
  113.9 1.7 %copy.24 = bf16[64,2048]{1,0:T(8,128)(2,1)} copy(bf16[64,2048]{1,0:T(8,128)(2,1)} %moe_exchange.1) | data formatting | bytes 524288
  (4 shorter events, 0.0 us)
Async XLA Ops:
  0.0 0.7 copy-start
